TPU v7x, 32 devices: a whole 2x2x4 slice. The times are simulated.
32 devices in a mesh: sp: 8 (over z, y), tp: 4 (over x, core).
Axes of the slice: x: 2, y: 2, z: 4, core: 2. Of those that a mesh axis runs over, the one named last changes fastest.
Arguments:
- inputs: bfloat16 [8, 6144, 2048], P(None, ('sp', 'tp')), may hold values from -6 to 6
- norm_gain: bfloat16 [2048], replicated, may hold values from 0.099609375 to 1.8984375
- key_weight: bfloat16 [2048, 512], replicated, may hold values from -0.125 to 0.125
- value_weight: bfloat16 [2048, 512], replicated, may hold values from -0.125 to 0.125
- query: bfloat16 [8, 1024], P('sp', 'tp'), may hold values from -15 to 15
- head_bias: bfloat16 [16], P('tp'), may hold values from -14 to -6
Outputs:
- key_cache: bfloat16 [8, 6144, 512], P('sp', None, 'tp')
- value_cache: bfloat16 [8, 6144, 512], P('sp', None, 'tp')
- first_read: bfloat16 [8, 1024], P('sp', 'tp')
All inputs are finite; a program needn't handle non-finite values.
Results may differ from a plain program's by a relative error of at most 0.012.
Values may be sent and summed in bfloat16 or wider, within the bound.
A program may use at most 128 MiB of HBM per device.

v0:
```python
import jax
import jax.numpy as jnp
from jax import lax
from jax.sharding import PartitionSpec as P

HEAD_DIMENSION = 64
EPSILON = 1e-06


def body(inputs, norm_gain, key_weight, value_weight, query, head_bias):
    groups = lax.axis_size("tp")
    seq_count, span_len, model_width = inputs.shape
    head_cols = key_weight.shape[1] // groups
    kv_heads = head_cols // HEAD_DIMENSION
    q_heads = query.shape[1] // HEAD_DIMENSION
    repeat = q_heads // kv_heads
    widened = inputs.astype(jnp.float32)
    normed = widened * lax.rsqrt(jnp.mean(widened * widened, axis=-1, keepdims=True) + EPSILON)
    normed = (normed * norm_gain.astype(jnp.float32)).astype(jnp.bfloat16)
    key_rows = jnp.einsum(
        "kru,uao->karo",
        normed,
        key_weight.reshape(model_width, groups, head_cols),
        preferred_element_type=jnp.float32,
    ).astype(jnp.bfloat16)
    value_rows = jnp.einsum(
        "kru,uao->karo",
        normed,
        value_weight.reshape(model_width, groups, head_cols),
        preferred_element_type=jnp.float32,
    ).astype(jnp.bfloat16)
    key_cache, value_cache = (
        lax.all_to_all(
            key_rows.reshape(seq_count * groups, span_len, head_cols),
            ("sp", "tp"),
            split_axis=0,
            concat_axis=1,
            tiled=True,
        ),
        lax.all_to_all(
            value_rows.reshape(seq_count * groups, span_len, head_cols),
            ("sp", "tp"),
            split_axis=0,
            concat_axis=1,
            tiled=True,
        ),
    )
    seq_len = key_cache.shape[1]
    query_tensor = query.reshape(kv_heads, repeat, HEAD_DIMENSION)
    key_tensor = key_cache.reshape(seq_len, kv_heads, HEAD_DIMENSION)
    value_tensor = value_cache.reshape(seq_len, kv_heads, HEAD_DIMENSION)
    score_logits = jnp.einsum(
        "ebx,uex->ebu", query_tensor, key_tensor, preferred_element_type=jnp.float32
    )
    score_logits = score_logits * HEAD_DIMENSION ** (-0.5) + head_bias.astype(jnp.float32).reshape(
        kv_heads, repeat, 1
    )
    log_keep = jax.nn.log_sigmoid(-score_logits)
    suffix_logs = lax.cumsum(log_keep, axis=2, reverse=True) - log_keep
    stick_weights = jnp.exp(jax.nn.log_sigmoid(score_logits) + suffix_logs).astype(jnp.bfloat16)
    attended_output = jnp.einsum(
        "euq,qec->euc", stick_weights, value_tensor, preferred_element_type=jnp.float32
    )
    first_read = attended_output.reshape(1, q_heads * HEAD_DIMENSION).astype(jnp.bfloat16)
    return (key_cache, value_cache, first_read)


def solution(mesh):
    placed = (P(None, ("sp", "tp"), None), P(), P(), P(), P("sp", "tp"), P("tp"))
    return jax.shard_map(
        body,
        mesh=mesh,
        in_specs=placed,
        out_specs=(P("sp", None, "tp"), P("sp", None, "tp"), P("sp", "tp")),
        check_vma=False,
    )
```

profile of v0, /device:TPU:0, one launch (start us, length us, event | category | flops | bytes accessed | tf_op | source)
XLA Modules:
  0.0 114.2 jit_solution(8614409717820748399)
XLA Ops:
  0.6 0.0 copy-start
  0.6 0.0 copy-start.1
  0.7 0.0 copy-start.2
  0.7 4.2 %fusion = f32[8,192]{1,0:T(8,128)S(1)} fusion(bf16[8,192,2048]{2,1,0:T(8,128)(2,1)} %param.6), kind=kLoop, calls=%fused_computation.2 | loop fusion | flops 9435648 | bytes 6297600 | tf_op jit(solution)/shard_map/reduce_sum | solution.py:18
  4.9 0.0 copy-done.2
  4.9 0.0 copy-done
  5.0 0.9 copy-done.1
  5.9 4.6 %fusion.12 = bf16[8,192,4,128]{3,1,2,0:T(8,128)(2,1)} fusion(bf16[8,192,2048]{2,1,0:T(8,128)(2,1)S(1)} %copy-done.1, f32[2048]{0:T(1024)S(1)} %convert_element_type.40, f32[8,192]{1,0:T(8,128)S(1)} %add_rsqrt_fusion, bf16[2048,512]{1,0:T(8,128)(2,1)S(1)} %copy-done), kind=kOutput, calls=%fused_computation.15 | convolution fusion | flops 3234594816 | bytes 9975808 | tf_op jit(solution)/shard_map/kru,uao->karo/dot_general | solution.py:20
  10.5 7.4 %all-to-all-start = ((bf16[32,192,128]{2,1,0:T(8,128)(2,1)}), bf16[32,192,128]{2,1,0:T(8,128)(2,1)}, u32[]{:S(2)}, u32[]{:S(2)}) async-start(bf16[32,192,128]{2,1,0:T(8,128)(2,1)} %bitcast.58), calls=%async_computation | async-start | bytes 3145728 | tf_op jit(solution)/shard_map/all_to_all | solution.py:33
  17.9 8.2 %fusion.15 = bf16[8,192,4,128]{3,1,2,0:T(8,128)(2,1)} fusion(bf16[8,192,2048]{2,1,0:T(8,128)(2,1)} %param.6, f32[2048]{0:T(1024)S(1)} %convert_element_type.40, f32[8,192]{1,0:T(8,128)S(1)} %add_rsqrt_fusion, bf16[2048,512]{1,0:T(8,128)(2,1)} %param.9), kind=kOutput, calls=%fused_computation.16 | convolution fusion | flops 3234594816 | bytes 9975808 | tf_op jit(solution)/shard_map/kru,uao->karo/dot_general | solution.py:26
  26.1 29.4 %all-to-all-done = bf16[32,192,128]{2,1,0:T(8,128)(2,1)} async-done(((bf16[32,192,128]{2,1,0:T(8,128)(2,1)}), bf16[32,192,128]{2,1,0:T(8,128)(2,1)}, u32[]{:S(2)}, u32[]{:S(2)}) %all-to-all-start) | async-done | bytes 1572896 | tf_op jit(solution)/shard_map/all_to_all | solution.py:33
  55.6 4.1 %all-to-all-start.1 = ((bf16[32,192,128]{2,1,0:T(8,128)(2,1)}), bf16[32,192,128]{2,1,0:T(8,128)(2,1)}, u32[]{:S(2)}, u32[]{:S(2)}) async-start(bf16[32,192,128]{2,1,0:T(8,128)(2,1)} %bitcast.57), calls=%async_computation.1 | async-start | bytes 3145728 | tf_op jit(solution)/shard_map/all_to_all | solution.py:40
  59.7 0.0 copy-done.3
  59.7 0.1 reshape.75
  59.8 0.1 reshape.79
  59.9 4.5 %copy.21 = bf16[32,192,128]{1,0,2:T(8,128)(2,1)} copy(bf16[32,192,128]{2,1,0:T(8,128)(2,1)} %all-to-all-done) | data formatting | bytes 3145728 | tf_op jit(solution)/shard_map/all_to_all | solution.py:33
  64.4 4.5 %reshape.74 = bf16[6144,2,64]{0,2,1:T(8,128)(2,1)} reshape(bf16[32,192,128]{1,0,2:T(8,128)(2,1)} %copy.21) | data formatting | bytes 3145728 | tf_op jit(solution)/shard_map/reshape | solution.py:50
  68.9 1.8 %fusion.21 = (f32[2,2,6144]{2,1,0:T(2,128)S(1)}, f32[2,2,6144]{2,1,0:T(2,128)S(1)}) fusion(f32[2,2]{1,0:T(2,128)S(1)} %reshape.79, bf16[6144,2,64]{0,2,1:T(8,128)(2,1)} %reshape.74, bf16[2,2,64]{2,1,0:T(2,128)(2,1)S(1)} %reshape.75), kind=kOutput, calls=%fused_computation.23 | convolution fusion | flops 3366912 | bytes 1770000 | tf_op jit(solution)/shard_map/ebx,uex->ebu/dot_general | solution.py:52
  70.7 0.1 reshape.76
  70.8 5.0 %reduce-window.6 = f32[2,2,48,128]{3,2,1,0:T(8,128)S(1)} reduce-window(f32[2,2,48,128]{3,2,1,0:T(8,128)S(1)} %reshape.76, f32[]{:T(128)} %constant.6.clone.1), window={size=1x1x1x128 pad=0_0x0_0x0_0x0_127}, to_apply=%region_1.2 | reduce-window | flops 3121152 | bytes 196612 | tf_op jit(solution)/shard_map/reduce-window
  75.9 0.1 slice_reduce_fusion
  76.0 0.7 reduce-window.9
  76.6 0.1 slice.9
  76.7 0.1 broadcast_add_fusion
  76.8 0.1 reduce_window_sum.15
  76.9 20.3 %all-to-all-done.1 = bf16[32,192,128]{2,1,0:T(8,128)(2,1)} async-done(((bf16[32,192,128]{2,1,0:T(8,128)(2,1)}), bf16[32,192,128]{2,1,0:T(8,128)(2,1)}, u32[]{:S(2)}, u32[]{:S(2)}) %all-to-all-start.1) | async-done | bytes 1572896 | tf_op jit(solution)/shard_map/all_to_all | solution.py:40
  97.2 4.5 %copy.22 = bf16[32,192,128]{1,0,2:T(8,128)(2,1)} copy(bf16[32,192,128]{2,1,0:T(8,128)(2,1)} %all-to-all-done.1) | data formatting | bytes 3145728 | tf_op jit(solution)/shard_map/all_to_all | solution.py:40
  101.7 4.5 %reshape.78 = bf16[6144,2,64]{0,2,1:T(8,128)(2,1)} reshape(bf16[32,192,128]{1,0,2:T(8,128)(2,1)} %copy.22) | data formatting | bytes 3145728 | tf_op jit(solution)/shard_map/reshape | solution.py:51
  106.2 2.1 %convolution_convert_fusion = bf16[2,2,64]{2,1,0:T(2,128)(2,1)S(1)} fusion(bf16[6144,2,64]{0,2,1:T(8,128)(2,1)} %reshape.78, f32[2,2,6144]{2,1,0:T(2,128)S(1)} %reduce_window_sum.15, f32[2,2,6144]{2,1,0:T(2,128)S(1)} %get-tuple-element.4), kind=kOutput, calls=%fused_computation.17 | convolution fusion | flops 3588352 | bytes 1769984 | tf_op jit(solution)/shard_map/euq,qec->euc/dot_general | solution.py:61
  108.3 0.7 convert_element_type.48
  108.9 2.7 %copy.40 = bf16[1,6144,128]{2,1,0:T(8,128)(2,1)} copy(bf16[1,6144,128]{2,1,0:T(8,128)(2,1)} %bitcast.5) | data formatting | bytes 3145728
  111.6 2.7 %copy.41 = bf16[1,6144,128]{2,1,0:T(8,128)(2,1)} copy(bf16[1,6144,128]{2,1,0:T(8,128)(2,1)} %bitcast.10) | data formatting | bytes 3145728
  (6 shorter events, 0.0 us)
Async XLA Ops:
  0.6 4.3 %copy-start = (bf16[2048,512]{1,0:T(8,128)(2,1)S(1)}, bf16[2048,512]{1,0:T(8,128)(2,1)}, u32[]{:S(2)}) copy-start(bf16[2048,512]{1,0:T(8,128)(2,1)} %param.8) | copy-start | bytes 6291460
  0.6 5.2 %copy-start.1 = (bf16[8,192,2048]{2,1,0:T(8,128)(2,1)S(1)}, bf16[8,192,2048]{2,1,0:T(8,128)(2,1)}, u32[]{:S(2)}) copy-start(bf16[8,192,2048]{2,1,0:T(8,128)(2,1)} %param.6) | copy-start | bytes 18874372
  0.7 4.3 %copy-start.2 = (bf16[2048]{0:T(1024)(128)(2,1)S(1)}, bf16[2048]{0:T(1024)(128)(2,1)}, u32[]{:S(2)}) copy-start(bf16[2048]{0:T(1024)(128)(2,1)} %param.7) | copy-start | bytes 12292
  10.5 45.1 %all-to-all-start = ((bf16[32,192,128]{2,1,0:T(8,128)(2,1)}), bf16[32,192,128]{2,1,0:T(8,128)(2,1)}, u32[]{:S(2)}, u32[]{:S(2)}) async-start(bf16[32,192,128]{2,1,0:T(8,128)(2,1)} %bitcast.58), calls=%async_computation | async-start | bytes 3145728 | tf_op jit(solution)/shard_map/all_to_all | solution.py:33
  26.1 33.5 %copy-start.3 = (bf16[1,256]{1,0:T(2,128)(2,1)S(1)}, bf16[1,256]{1,0:T(2,128)(2,1)}, u32[]{:S(2)}) copy-start(bf16[1,256]{1,0:T(2,128)(2,1)} %param.10) | copy-start | bytes 1540
  26.1 33.7 %copy-start.4 = (bf16[4]{0:T(256)(128)(2,1)S(1)}, bf16[4]{0:T(256)(128)(2,1)}, u32[]{:S(2)}) copy-start(bf16[4]{0:T(256)(128)(2,1)} %param.11) | copy-start | bytes 28
  55.6 41.6 %all-to-all-start.1 = ((bf16[32,192,128]{2,1,0:T(8,128)(2,1)}), bf16[32,192,128]{2,1,0:T(8,128)(2,1)}, u32[]{:S(2)}, u32[]{:S(2)}) async-start(bf16[32,192,128]{2,1,0:T(8,128)(2,1)} %bitcast.57), calls=%async_computation.1 | async-start | bytes 3145728 | tf_op jit(solution)/shard_map/all_to_all | solution.py:40
where the time goes:
time: 115 us; the launch traced here: 114 us
  waiting for transfers between devices  49.8 us (43%)
  local copies, waits for them, and re-layouts  25.4 us (22%)
  matrix products  16.7 us (15%)
  starting transfers between devices  11.5 us (10%)
  other arithmetic  10.1 us (9%)
    all_to_all x1, waiting for transfers between devices, body(): lax.all_to_all(key_rows.reshape(seq_count * groups, span_len, head_cols),...  29.4 us
    all_to_all x1, waiting for transfers between devices, body(): lax.all_to_all(value_rows.reshape(seq_count * groups, span_len, head_cols...  20.3 us
    dot_general x1, matrix products, body(): jnp.einsum('kru,uao->karo', normed, value_weight.reshape(model_width, gro...  8.19 us
    all_to_all x1, starting transfers between devices, body(): lax.all_to_all(key_rows.reshape(seq_count * groups, span_len, head_cols),...  7.43 us
    unnamed x12, local copies, waits for them, and re-layouts  6.27 us
    another operation x2, other arithmetic  5.69 us
    dot_general x1, matrix products, body(): jnp.einsum('kru,uao->karo', normed, key_weight.reshape(model_width, group...  4.62 us
    all_to_all x1, local copies, waits for them, and re-layouts, body(): lax.all_to_all(key_rows.reshape(seq_count * groups, span_len, head_cols),...  4.53 us
  transfers between devices with their start and end apart: 2, of which 2 were waited for; matrix products, arithmetic and copies ran while one was open for 22% of the time, Pallas kernels for 0%

commit v1 on v0

--- a/solution.py
+++ b/solution.py
@@ -37,12 +37,20 @@
             concat_axis=1,
             tiled=True,
         ),
-        lax.all_to_all(
-            value_rows.reshape(seq_count * groups, span_len, head_cols),
-            ("sp", "tp"),
-            split_axis=0,
-            concat_axis=1,
-            tiled=True,
+        jnp.concatenate(
+            lax.all_to_all(
+                jnp.stack(
+                    jnp.split(
+                        value_rows.reshape(seq_count * groups, span_len, head_cols),
+                        lax.axis_size(("sp", "tp")),
+                        axis=0,
+                    )
+                ),
+                ("sp", "tp"),
+                0,
+                0,
+            ),
+            axis=1,
         ),
     )
     seq_len = key_cache.shape[1]

time: 115 us -> 142 us (1.23)
  local copies, waits for them, and re-layouts: 25.4 us -> 45.4 us
  waiting for transfers between devices: 49.8 us -> 57.7 us
    unnamed x12 -> x43, local copies, waits for them, and re-layouts: 6.27 us -> 25.6 us
    all_to_all x1, waiting for transfers between devices: 20.3 us -> 29.4 us  [body(): lax.all_to_all(jnp.stack(jnp.split(value_rows.reshape(seq_count * groups,...]
    another operation x1 -> x3, local copies, waits for them, and re-layouts: 0.08 us -> 5.18 us  [the longest x1 4.49 us: body(): value_tensor = value_cache.reshape(seq_len, kv_heads, HEAD_DIMENSION)]
    reshape x2 -> x1, local copies, waits for them, and re-layouts: 4.57 us -> 0.08 us  [the longest x1 4.49 us: body(): value_tensor = value_cache.reshape(seq_len, kv_heads, HEAD_DIMENSION)]
    dot_general x1, matrix products: 8.19 us -> 3.73 us  [body(): jnp.einsum('kru,uao->karo', normed, value_weight.reshape(model_width, gro...]
    dot_general x1, matrix products: 4.62 us -> 8.19 us  [body(): jnp.einsum('kru,uao->karo', normed, key_weight.reshape(model_width, group...]
    all_to_all x1, starting transfers between devices: 4.1 us -> 7.43 us  [body(): lax.all_to_all(jnp.stack(jnp.split(value_rows.reshape(seq_count * groups,...]
    all_to_all x1, starting transfers between devices: 7.43 us -> 4.1 us  [body(): lax.all_to_all(key_rows.reshape(seq_count * groups, span_len, head_cols),...]
  transfers between devices with their start and end apart: 2 -> 2, of which waited for: 2 -> 2; matrix products, arithmetic and copies ran while one was open for 22% -> 12% of each run, Pallas kernels for 0% -> 0%
where the time goes in v1:
time: 142 us; the launch traced here: 141 us
  waiting for transfers between devices  57.7 us (41%)
  local copies, waits for them, and re-layouts  45.4 us (32%)
  matrix products  15.8 us (11%)
  starting transfers between devices  11.5 us (8%)
  other arithmetic  10.1 us (7%)
    all_to_all x1, waiting for transfers between devices, body(): lax.all_to_all(jnp.stack(jnp.split(value_rows.reshape(seq_count * groups,...  29.4 us
    all_to_all x1, waiting for transfers between devices, body(): lax.all_to_all(key_rows.reshape(seq_count * groups, span_len, head_cols),...  28.3 us
    unnamed x43, local copies, waits for them, and re-layouts  25.6 us
    dot_general x1, matrix products, body(): jnp.einsum('kru,uao->karo', normed, key_weight.reshape(model_width, group...  8.19 us
    all_to_all x1, starting transfers between devices, body(): lax.all_to_all(jnp.stack(jnp.split(value_rows.reshape(seq_count * groups,...  7.43 us
    another operation x2, other arithmetic  5.69 us
    all_to_all x1, local copies, waits for them, and re-layouts, body(): lax.all_to_all(jnp.stack(jnp.split(value_rows.reshape(seq_count * groups,...  4.53 us
    all_to_all x1, local copies, waits for them, and re-layouts, body(): lax.all_to_all(key_rows.reshape(seq_count * groups, span_len, head_cols),...  4.53 us
  transfers between devices with their start and end apart: 2, of which 2 were waited for; matrix products, arithmetic and copies ran while one was open for 12% of the time, Pallas kernels for 0%

profile of v1, /device:TPU:0, one launch (start us, length us, event | category | flops | bytes accessed | tf_op | source)
XLA Modules:
  0.0 141.3 jit_solution(17634408036178562669)
XLA Ops:
  0.7 4.2 %fusion = f32[8,192]{1,0:T(8,128)S(1)} fusion(bf16[8,192,2048]{2,1,0:T(8,128)(2,1)} %param.6), kind=kLoop, calls=%fused_computation.2 | loop fusion | flops 9435648 | bytes 6297600 | tf_op jit(solution)/shard_map/reduce_sum | solution.py:18
  5.0 0.9 copy-done.1
  5.9 3.7 %fusion.15 = bf16[8,192,4,128]{3,1,2,0:T(8,128)(2,1)S(1)} fusion(bf16[8,192,2048]{2,1,0:T(8,128)(2,1)S(1)} %copy-done.1, f32[2048]{0:T(1024)S(1)} %convert_element_type.40, f32[8,192]{1,0:T(8,128)S(1)} %add_rsqrt_fusion, bf16[2048,512]{1,0:T(8,128)(2,1)S(1)} %copy-done), kind=kOutput, calls=%fused_computation.16 | convolution fusion | flops 3234594816 | bytes 9975808 | tf_op jit(solution)/shard_map/kru,uao->karo/dot_general | solution.py:26
  9.6 0.6 constant_dynamic-update-slice_fusion.31
  10.3 0.6 constant_dynamic-update-slice_fusion.30
  11.5 0.6 constant_dynamic-update-slice_fusion.28
  12.1 0.6 constant_dynamic-update-slice_fusion.27
  12.7 0.6 constant_dynamic-update-slice_fusion.26
  13.4 0.6 constant_dynamic-update-slice_fusion.25
  14.6 0.6 constant_dynamic-update-slice_fusion.23
  15.2 0.6 constant_dynamic-update-slice_fusion.22
  15.9 0.6 constant_dynamic-update-slice_fusion.21
  16.5 0.6 constant_dynamic-update-slice_fusion.20
  17.1 0.6 constant_dynamic-update-slice_fusion.19
  17.7 0.6 constant_dynamic-update-slice_fusion.18
  18.4 0.6 constant_dynamic-update-slice_fusion.17
  29.6 7.4 %all-to-all-start.1 = ((bf16[32,1,192,128]{3,2,1,0:T(8,128)(2,1)}), bf16[32,1,192,128]{3,2,1,0:T(8,128)(2,1)}, u32[]{:S(2)}, u32[]{:S(2)}) async-start(bf16[32,1,192,128]{3,2,1,0:T(8,128)(2,1)} %constant_dynamic-update-slice_fusion), calls=%async_computation.1 | async-start | bytes 3145728 | tf_op jit(solution)/shard_map/all_to_all | solution.py:41
  37.0 8.2 %fusion.12 = bf16[8,192,4,128]{3,1,2,0:T(8,128)(2,1)} fusion(bf16[8,192,2048]{2,1,0:T(8,128)(2,1)} %param.6, f32[2048]{0:T(1024)S(1)} %convert_element_type.40, f32[8,192]{1,0:T(8,128)S(1)} %add_rsqrt_fusion, bf16[2048,512]{1,0:T(8,128)(2,1)} %param.8), kind=kOutput, calls=%fused_computation.15 | convolution fusion | flops 3234594816 | bytes 9975808 | tf_op jit(solution)/shard_map/kru,uao->karo/dot_general | solution.py:20
  45.2 29.4 %all-to-all-done.1 = bf16[32,1,192,128]{3,2,1,0:T(8,128)(2,1)} async-done(((bf16[32,1,192,128]{3,2,1,0:T(8,128)(2,1)}), bf16[32,1,192,128]{3,2,1,0:T(8,128)(2,1)}, u32[]{:S(2)}, u32[]{:S(2)}) %all-to-all-start.1) | async-done | bytes 1572896 | tf_op jit(solution)/shard_map/all_to_all | solution.py:41
  74.7 4.1 %all-to-all-start = ((bf16[32,192,128]{2,1,0:T(8,128)(2,1)}), bf16[32,192,128]{2,1,0:T(8,128)(2,1)}, u32[]{:S(2)}, u32[]{:S(2)}) async-start(bf16[32,192,128]{2,1,0:T(8,128)(2,1)} %bitcast.187), calls=%async_computation | async-start | bytes 3145728 | tf_op jit(solution)/shard_map/all_to_all | solution.py:33
  79.0 4.5 %copy.58 = bf16[32,1,192,128]{2,0,3,1:T(8,128)(2,1)} copy(bf16[32,1,192,128]{3,2,1,0:T(8,128)(2,1)} %all-to-all-done.1) | data formatting | bytes 3145728 | tf_op jit(solution)/shard_map/all_to_all | solution.py:41
  83.5 4.5 %reshape_reshape.3 = bf16[6144,2,64]{0,2,1:T(8,128)(2,1)} reshape(bf16[32,1,192,128]{2,0,3,1:T(8,128)(2,1)} %copy.58) | data formatting | bytes 3145728 | tf_op jit(solution)/shard_map/reshape;reshape | solution.py:59
  88.0 28.3 %all-to-all-done = bf16[32,192,128]{2,1,0:T(8,128)(2,1)} async-done(((bf16[32,192,128]{2,1,0:T(8,128)(2,1)}), bf16[32,192,128]{2,1,0:T(8,128)(2,1)}, u32[]{:S(2)}, u32[]{:S(2)}) %all-to-all-start) | async-done | bytes 1572896 | tf_op jit(solution)/shard_map/all_to_all | solution.py:33
  116.3 4.5 %copy.57 = bf16[32,192,128]{1,0,2:T(8,128)(2,1)} copy(bf16[32,192,128]{2,1,0:T(8,128)(2,1)} %all-to-all-done) | data formatting | bytes 3145728 | tf_op jit(solution)/shard_map/all_to_all | solution.py:33
  120.8 4.5 %reshape.71 = bf16[6144,2,64]{0,2,1:T(8,128)(2,1)} reshape(bf16[32,192,128]{1,0,2:T(8,128)(2,1)} %copy.57) | data formatting | bytes 3145728 | tf_op jit(solution)/shard_map/reshape | solution.py:58
  125.3 1.8 %fusion.21 = (f32[2,2,6144]{2,1,0:T(2,128)S(1)}, f32[2,2,6144]{2,1,0:T(2,128)S(1)}) fusion(f32[2,2]{1,0:T(2,128)S(1)} %reshape.75, bf16[6144,2,64]{0,2,1:T(8,128)(2,1)} %reshape.71, bf16[2,2,64]{2,1,0:T(2,128)(2,1)S(1)} %reshape.72), kind=kOutput, calls=%fused_computation.23 | convolution fusion | flops 3366912 | bytes 1770000 | tf_op jit(solution)/shard_map/ebx,uex->ebu/dot_general | solution.py:60
  127.2 5.0 %reduce-window.6 = f32[2,2,48,128]{3,2,1,0:T(8,128)S(1)} reduce-window(f32[2,2,48,128]{3,2,1,0:T(8,128)S(1)} %reshape.73, f32[]{:T(128)} %constant.6.clone.1), window={size=1x1x1x128 pad=0_0x0_0x0_0x0_127}, to_apply=%region_1.2 | reduce-window | flops 3121152 | bytes 196612 | tf_op jit(solution)/shard_map/reduce-window
  132.3 0.7 reduce-window.9
  133.2 2.1 %convolution_convert_fusion = bf16[2,2,64]{2,1,0:T(2,128)(2,1)S(1)} fusion(bf16[6144,2,64]{0,2,1:T(8,128)(2,1)} %reshape_reshape.3, f32[2,2,6144]{2,1,0:T(2,128)S(1)} %reduce_window_sum.15, f32[2,2,6144]{2,1,0:T(2,128)S(1)} %get-tuple-element.4), kind=kOutput, calls=%fused_computation.17 | convolution fusion | flops 3588352 | bytes 1769984 | tf_op jit(solution)/shard_map/euq,qec->euc/dot_general | solution.py:69
  135.3 0.7 convert_element_type.48
  136.0 2.7 %copy.107 = bf16[1,6144,128]{2,1,0:T(8,128)(2,1)} copy(bf16[1,6144,128]{2,1,0:T(8,128)(2,1)} %bitcast.5) | data formatting | bytes 3145728
  138.6 2.7 %copy.108 = bf16[1,6144,128]{2,1,0:T(8,128)(2,1)} copy(bf16[1,6144,128]{2,1,0:T(8,128)(2,1)} %bitcast.43) | data formatting | bytes 3145728
  (38 shorter events, 12.5 us)
Async XLA Ops:
  0.6 4.3 %copy-start = (bf16[2048,512]{1,0:T(8,128)(2,1)S(1)}, bf16[2048,512]{1,0:T(8,128)(2,1)}, u32[]{:S(2)}) copy-start(bf16[2048,512]{1,0:T(8,128)(2,1)} %param.9) | copy-start | bytes 6291460
  0.6 5.2 %copy-start.1 = (bf16[8,192,2048]{2,1,0:T(8,128)(2,1)S(1)}, bf16[8,192,2048]{2,1,0:T(8,128)(2,1)}, u32[]{:S(2)}) copy-start(bf16[8,192,2048]{2,1,0:T(8,128)(2,1)} %param.6) | copy-start | bytes 18874372
  0.7 4.3 %copy-start.2 = (bf16[2048]{0:T(1024)(128)(2,1)S(1)}, bf16[2048]{0:T(1024)(128)(2,1)}, u32[]{:S(2)}) copy-start(bf16[2048]{0:T(1024)(128)(2,1)} %param.7) | copy-start | bytes 12292
  29.6 45.1 %all-to-all-start.1 = ((bf16[32,1,192,128]{3,2,1,0:T(8,128)(2,1)}), bf16[32,1,192,128]{3,2,1,0:T(8,128)(2,1)}, u32[]{:S(2)}, u32[]{:S(2)}) async-start(bf16[32,1,192,128]{3,2,1,0:T(8,128)(2,1)} %constant_dynamic-update-slice_fusion), calls=%async_computation.1 | async-start | bytes 3145728 | tf_op jit(solution)/shard_map/all_to_all | solution.py:41
  74.7 4.1 %copy-start.3 = (bf16[1,256]{1,0:T(2,128)(2,1)S(1)}, bf16[1,256]{1,0:T(2,128)(2,1)}, u32[]{:S(2)}) copy-start(bf16[1,256]{1,0:T(2,128)(2,1)} %param.10) | copy-start | bytes 1540
  74.7 4.2 %copy-start.4 = (bf16[4]{0:T(256)(128)(2,1)S(1)}, bf16[4]{0:T(256)(128)(2,1)}, u32[]{:S(2)}) copy-start(bf16[4]{0:T(256)(128)(2,1)} %param.11) | copy-start | bytes 28
  74.7 41.6 %all-to-all-start = ((bf16[32,192,128]{2,1,0:T(8,128)(2,1)}), bf16[32,192,128]{2,1,0:T(8,128)(2,1)}, u32[]{:S(2)}, u32[]{:S(2)}) async-start(bf16[32,192,128]{2,1,0:T(8,128)(2,1)} %bitcast.187), calls=%async_computation | async-start | bytes 3145728 | tf_op jit(solution)/shard_map/all_to_all | solution.py:33
